TPU v7x, 32 devices: a whole 2x2x4 slice. The times are simulated.
32 devices in a mesh: grp: 2 (over y), sp: 4 (over z), tp: 4 (over x, core).
Axes of the slice: x: 2, y: 2, z: 4, core: 2. Of those that a mesh axis runs over, the one named last changes fastest.
Arguments:
- tokens: bfloat16 [3072, 2048], P(('grp', 'sp'), 'tp'), parts along dimension 0, may hold values from -15 to 15
- gate_weight: bfloat16 [2, 2048, 2048], P(None, 'sp', 'tp'), may hold values from -0.125 to 0.125
- inner_weight: bfloat16 [2, 2048, 2048], P(None, 'sp', 'tp'), may hold values from -0.125 to 0.125
- value_weight: bfloat16 [2, 2048, 2048], P(None, 'sp', 'tp'), may hold values from -0.125 to 0.125
- out_weight: bfloat16 [2, 2048, 2048], P(None, 'tp', 'sp'), may hold values from -0.125 to 0.125
- taps: bfloat16 [2, 3, 2048], P(None, None, 'tp'), may hold values from -3 to 3
- norm_gain: float32 [2, 2048], P(None, 'tp'), may hold values from 0.1 to 1.9
- norm_bias: float32 [2, 2048], P(None, 'tp'), may hold values from -1.5 to 1.5
Outputs:
- mixed: bfloat16 [3072, 2048], P(('grp', 'sp'), 'tp'), parts along dimension 0
There are 2 independent parts, one for each index of `grp`. A program takes and returns all parts, laid end to end along the dimension named above; an argument that names none is the same for every part. Nothing has to cross between parts.
All inputs are finite; a program needn't handle non-finite values.
Results may differ from a plain program's by a relative error of at most 0.03.
Values may be sent and summed in bfloat16 or wider, within the bound.
No kernel may reach another device: no remote copies, remote signals or barrier semaphores. Data moves between devices by JAX's collectives and lax.ppermute only.
A program may use at most 64 MiB of HBM per device.

v0:
```python
import jax
import jax.numpy as jnp
from jax import lax
from jax.sharding import PartitionSpec as P

LAYERS = 2


def extended(value, sides, width):
    for axis, dim in sides:
        peers, length = (lax.axis_size(axis), value.shape[dim])
        up = [(i, (i + 1) % peers) for i in range(peers - 1)]
        down = [(j, i) for i, j in up]
        last = lax.slice_in_dim(value, length - width, length, axis=dim)
        initial = lax.slice_in_dim(value, 0, width, axis=dim)
        before = lax.ppermute(last, axis, up)
        after = lax.ppermute(initial, axis, down)
        value = jnp.concatenate([before, value, after], axis=dim)
    return value


def shards(tokens, gate_weight, inner_weight, value_weight, out_weight, taps, norm_gain, norm_bias):
    x = tokens
    width = x.shape[1] * lax.axis_size("tp")
    full_gate, full_inner, full_value, full_out = (
        lax.all_gather(gate_weight, "sp", axis=1, tiled=True),
        lax.all_gather(inner_weight, "sp", axis=1, tiled=True),
        lax.all_gather(value_weight, "sp", axis=1, tiled=True),
        lax.all_gather(out_weight, "sp", axis=2, tiled=True),
    )
    for layer in range(LAYERS):
        whole = lax.all_gather(x, "tp", axis=1, tiled=True)
        outer = jnp.dot(whole, full_gate[layer], preferred_element_type=jnp.float32)
        inner = jnp.dot(whole, full_inner[layer], preferred_element_type=jnp.float32)
        values = jnp.dot(whole, full_value[layer], preferred_element_type=jnp.float32)
        outer = outer.astype(jnp.bfloat16)
        inner = inner.astype(jnp.bfloat16)
        values = values.astype(jnp.bfloat16)
        product = (inner.astype(jnp.float32) * values.astype(jnp.float32)).astype(jnp.bfloat16)
        padded = extended(product, (("sp", 0),), 1).astype(jnp.float32)
        kernel = taps[layer].astype(jnp.float32)
        conv = kernel[0] * padded[:-2] + kernel[1] * padded[1:-1] + kernel[2] * padded[2:]
        gated = (outer.astype(jnp.float32) * conv).astype(jnp.bfloat16)
        terms = jnp.dot(gated, full_out[layer], preferred_element_type=jnp.float32)
        branch = lax.psum_scatter(
            terms.astype(jnp.bfloat16), "tp", scatter_dimension=1, tiled=True
        ).astype(jnp.float32)
        total = 2.0**0.5 * x.astype(jnp.float32) + branch
        row_sum, row_square = lax.psum(
            (jnp.sum(total, axis=1), jnp.sum(total * total, axis=1)), "tp"
        )
        mean = (row_sum / width)[:, None]
        spread = (row_square / width)[:, None] - mean * mean
        x = (
            (total - mean) * lax.rsqrt(spread + 1e-05) * norm_gain[layer] + norm_bias[layer]
        ).astype(jnp.bfloat16)
    return x


def solution(mesh):
    in_specs = (
        P(("grp", "sp"), "tp"),
        P(None, "sp", "tp"),
        P(None, "sp", "tp"),
        P(None, "sp", "tp"),
        P(None, "tp", "sp"),
        P(None, None, "tp"),
        P(None, "tp"),
        P(None, "tp"),
    )
    out_specs = P(("grp", "sp"), "tp")
    return jax.shard_map(shards, mesh=mesh, in_specs=in_specs, out_specs=out_specs, check_vma=False)
```

profile of v0, /device:TPU:0, one launch (start us, length us, event | category | flops | bytes accessed | tf_op | source)
XLA Modules:
  0.0 479.8 jit_solution(8200364497382368189)
XLA Ops:
  6.5 0.0 all-gather.7.cloned.1.call-start
  6.5 0.7 all-gather.7.cloned.1.call-update
  7.3 0.0 copy-start.2
  7.3 0.0 all-gather.13.cloned.1.call-start
  7.3 0.7 all-gather.13.cloned.1.call-update
  8.0 0.0 all-gather.11.cloned.1.call-start
  8.1 0.7 all-gather.11.cloned.1.call-update
  8.8 0.0 all-gather.15.cloned.1.call-start
  8.8 0.5 all-gather.15.cloned.1.call-update
  9.3 0.0 all-gather.9.cloned.1.call-start
  9.4 0.5 all-gather.9.cloned.1.call-update
  9.9 0.0 reduce-scatter.3.cloned.1.call-start
  10.0 0.0 copy-done.2
  10.0 21.3 %all-gather.7.cloned.1.call-done = bf16[384,2048]{1,0:T(8,128)(2,1)} async-done(((bf16[384,512]{1,0:T(8,128)(2,1)}), bf16[384,2048]{1,0:T(8,128)(2,1)}) %all-gather.7.cloned.1.call-update) | async-done | bytes 1572880 | tf_op jit(solution)/shard_map/all_gather | solution.py:32
  31.3 0.0 copy-start.6
  31.3 82.3 %all-gather.13.cloned.1.call-done = bf16[2,2048,512]{2,1,0:T(8,128)(2,1)} async-done(((bf16[2,512,512]{2,1,0:T(8,128)(2,1)}), bf16[2,2048,512]{2,1,0:T(8,128)(2,1)}) %all-gather.13.cloned.1.call-update) | async-done | bytes 4194320 | tf_op jit(solution)/shard_map/all_gather | solution.py:28
  113.6 3.0 fusion.15
  116.7 77.8 %all-gather.11.cloned.1.call-done = bf16[2,2048,512]{2,1,0:T(8,128)(2,1)} async-done(((bf16[2,512,512]{2,1,0:T(8,128)(2,1)}), bf16[2,2048,512]{2,1,0:T(8,128)(2,1)}) %all-gather.11.cloned.1.call-update) | async-done | bytes 4194320 | tf_op jit(solution)/shard_map/all_gather | solution.py:27
  194.5 0.0 copy-done.6
  194.5 2.6 fusion.13
  197.0 1.3 collective-permute-start
  198.3 1.3 collective-permute-start.1
  199.7 0.0 collective-permute-done
  199.7 4.2 collective-permute-done.1
  203.9 0.1 maximum_convert_fusion
  204.0 71.1 %all-gather.15.cloned.1.call-done = bf16[2,512,2048]{2,1,0:T(8,128)(2,1)} async-done(((bf16[2,512,512]{2,1,0:T(8,128)(2,1)}), bf16[2,512,2048]{2,1,0:T(8,128)(2,1)}) %all-gather.15.cloned.1.call-update) | async-done | bytes 4194320 | tf_op jit(solution)/shard_map/all_gather | solution.py:29
  275.1 80.7 %all-gather.9.cloned.1.call-done = bf16[2,2048,512]{2,1,0:T(8,128)(2,1)} async-done(((bf16[2,512,512]{2,1,0:T(8,128)(2,1)}), bf16[2,2048,512]{2,1,0:T(8,128)(2,1)}) %all-gather.9.cloned.1.call-update) | async-done | bytes 4194320 | tf_op jit(solution)/shard_map/all_gather | solution.py:26
  355.8 0.0 copy-start.3
  355.8 0.0 copy-start.4
  355.8 0.0 copy-start.1
  355.8 5.4 %convolution_convert_fusion.1 = bf16[384,2048]{1,0:T(8,128)(2,1)} fusion(bf16[2,512,2048]{2,1,0:T(8,128)(2,1)} %all-gather.15.cloned.1.call-done, bf16[384,2048]{1,0:T(8,128)(2,1)S(1)} %copy-done.6, bf16[2,2048,512]{2,1,0:T(8,128)(2,1)} %all-gather.9.cloned.1.call-done, f32[386,512]{1,0:T(8,128)S(1)} %maximum_convert_fusion, f32[512]{0:T(512)S(1)} %bitcast.92, ...), kind=kOutput, calls=%fused_computation.1 | convolution fusion | flops 1613168640 | bytes 9705472 | tf_op jit(solution)/shard_map/dot_general | solution.py:44
  361.2 0.0 reduce-scatter.3.cloned.1.call-update
  361.2 0.0 all-gather.17.cloned.1.call-start
  361.3 0.0 copy-done.3
  361.3 0.0 copy-done.4
  361.3 26.6 %reduce-scatter.3.cloned.1.call-done = bf16[384,512]{1,0:T(8,128)(2,1)} async-done(((bf16[384,2048]{1,0:T(8,128)(2,1)}), bf16[384,512]{1,0:T(8,128)(2,1)}) %reduce-scatter.3.cloned.1.call-update) | async-done | bytes 393232 | tf_op jit(solution)/shard_map/reduce_scatter | solution.py:45
  387.9 0.0 copy-done.1
  387.9 1.3 fusion.34
  389.2 5.8 %all-reduce.1 = (f32[384]{0:T(512)S(1)}, f32[384]{0:T(512)S(1)}) all-reduce(f32[384]{0:T(512)S(1)} %get-tuple-element.8, f32[384]{0:T(512)S(1)} %get-tuple-element.7), channel_id=1, replica_groups=mesh['grp'=2,'sp'=4,'tp'=4] {'tp'}, use_global_device_ids=true, to_apply=%region_4.0 | all-reduce | flops 768 | bytes 6144 | tf_op jit(solution)/shard_map/psum | solution.py:49
  395.0 2.0 add_convert_fusion.1
  397.0 0.0 all-gather.17.cloned.1.call-update
  397.0 0.0 reduce-scatter.5.cloned.1.call-start
  397.0 20.3 %all-gather.17.cloned.1.call-done = bf16[384,2048]{1,0:T(8,128)(2,1)} async-done(((bf16[384,512]{1,0:T(8,128)(2,1)}), bf16[384,2048]{1,0:T(8,128)(2,1)}) %all-gather.17.cloned.1.call-update) | async-done | bytes 1572880 | tf_op jit(solution)/shard_map/all_gather | solution.py:32
  417.4 0.0 copy-start.5
  417.4 0.0 copy-start.7
  417.4 3.2 fusion.25
  420.6 0.1 copy-done.5
  420.7 0.5 copy-done.7
  421.2 1.0 fusion.23
  422.2 3.4 collective-permute-start.2
  425.5 1.3 collective-permute-start.3
  426.8 0.0 collective-permute-done.2
  426.9 4.2 collective-permute-done.3
  431.0 0.1 maximum_convert_fusion.1
  431.1 0.0 copy-start
  431.2 5.5 %convolution_convert_fusion = bf16[384,2048]{1,0:T(8,128)(2,1)} fusion(bf16[2,512,2048]{2,1,0:T(8,128)(2,1)} %all-gather.15.cloned.1.call-done, bf16[384,2048]{1,0:T(8,128)(2,1)S(1)} %copy-done.7, bf16[2,2048,512]{2,1,0:T(8,128)(2,1)} %all-gather.9.cloned.1.call-done, f32[386,512]{1,0:T(8,128)S(1)} %maximum_convert_fusion.1, f32[512]{0:T(512)S(1)} %bitcast.89, ...), kind=kOutput, calls=%fused_computation | convolution fusion | flops 1613168640 | bytes 9705472 | tf_op jit(solution)/shard_map/dot_general | solution.py:44
  436.6 0.0 reduce-scatter.5.cloned.1.call-update
  436.7 27.3 %reduce-scatter.5.cloned.1.call-done = bf16[384,512]{1,0:T(8,128)(2,1)} async-done(((bf16[384,2048]{1,0:T(8,128)(2,1)}), bf16[384,512]{1,0:T(8,128)(2,1)}) %reduce-scatter.5.cloned.1.call-update) | async-done | bytes 393232 | tf_op jit(solution)/shard_map/reduce_scatter | solution.py:45
  464.0 0.0 copy-done
  464.0 1.3 fusion.35
  465.2 5.8 %all-reduce = (f32[384]{0:T(512)S(1)}, f32[384]{0:T(512)S(1)}) all-reduce(f32[384]{0:T(512)S(1)} %get-tuple-element.6, f32[384]{0:T(512)S(1)} %get-tuple-element.5), channel_id=1, replica_groups=mesh['grp'=2,'sp'=4,'tp'=4] {'tp'}, use_global_device_ids=true, to_apply=%region_9.0 | all-reduce | flops 768 | bytes 6144 | tf_op jit(solution)/shard_map/psum | solution.py:49
  471.0 2.0 add_convert_fusion
  (8 shorter events, 0.1 us)
Async XLA Ops:
  6.5 24.7 %all-gather.7.cloned.1.call-start = ((), (), s32[]{:S(2)}) async-start(), calls=%async_computation.2 | async-start | bytes 1966080 | tf_op jit(solution)/shard_map/all_gather | solution.py:32
  7.3 2.7 copy-start.2
  7.3 106.4 %all-gather.13.cloned.1.call-start = ((), (), s32[]{:S(2)}) async-start(), calls=%async_computation.5 | async-start | bytes 5242880 | tf_op jit(solution)/shard_map/all_gather | solution.py:28
  8.0 186.4 %all-gather.11.cloned.1.call-start = ((), (), s32[]{:S(2)}) async-start(), calls=%async_computation.4 | async-start | bytes 5242880 | tf_op jit(solution)/shard_map/all_gather | solution.py:27
  8.8 266.4 %all-gather.15.cloned.1.call-start = ((), (), s32[]{:S(2)}) async-start(), calls=%async_computation.6 | async-start | bytes 5242880 | tf_op jit(solution)/shard_map/all_gather | solution.py:29
  9.3 346.5 %all-gather.9.cloned.1.call-start = ((), (), s32[]{:S(2)}) async-start(), calls=%async_computation.3 | async-start | bytes 5242880 | tf_op jit(solution)/shard_map/all_gather | solution.py:26
  9.9 378.0 %reduce-scatter.3.cloned.1.call-start = ((), (), s32[]{:S(2)}) async-start(), calls=%async_computation.7 | async-start | bytes 1966080 | tf_op jit(solution)/shard_map/reduce_scatter | solution.py:45
  31.3 163.2 %copy-start.6 = (bf16[384,2048]{1,0:T(8,128)(2,1)S(1)}, bf16[384,2048]{1,0:T(8,128)(2,1)}, u32[]{:S(2)}) copy-start(bf16[384,2048]{1,0:T(8,128)(2,1)} %all-gather.7.cloned.1.call-done) | copy-start | bytes 4718596
  197.0 2.6 collective-permute-start
  198.3 5.6 %collective-permute-start.1 = (bf16[1,512]{1,0:T(2,128)(2,1)S(1)}, bf16[1,512]{1,0:T(2,128)(2,1)S(1)}, u32[]{:S(2)}, u32[]{:S(2)}) collective-permute-start(bf16[1,512]{1,0:T(2,128)(2,1)S(1)} %get-tuple-element.16), channel_id=1, source_target_pairs={{4,0},{8,4},{12,8},{5,1},{9,5},{13,9},{6,2},{10,6},{14,10},{7,3},{... | collective-permute-start | bytes 3080 | tf_op jit(solution)/shard_map/ppermute | solution.py:17
  355.8 5.5 %copy-start.3 = (f32[2,512]{1,0:T(2,128)S(1)}, f32[2,512]{1,0:T(2,128)}, u32[]{:S(2)}) copy-start(f32[2,512]{1,0:T(2,128)} %param.14) | copy-start | bytes 12292
  355.8 5.5 %copy-start.4 = (f32[2,512]{1,0:T(2,128)S(1)}, f32[2,512]{1,0:T(2,128)}, u32[]{:S(2)}) copy-start(f32[2,512]{1,0:T(2,128)} %param.15) | copy-start | bytes 12292
  355.8 32.1 %copy-start.1 = (bf16[384,512]{1,0:T(8,128)(2,1)S(1)}, bf16[384,512]{1,0:T(8,128)(2,1)}, u32[]{:S(2)}) copy-start(bf16[384,512]{1,0:T(8,128)(2,1)} %param.8) | copy-start | bytes 1179652
  361.2 56.1 %all-gather.17.cloned.1.call-start = ((), (), s32[]{:S(2)}) async-start(), calls=%async_computation.8 | async-start | bytes 1966080 | tf_op jit(solution)/shard_map/all_gather | solution.py:32
  397.0 67.0 %reduce-scatter.5.cloned.1.call-start = ((), (), s32[]{:S(2)}) async-start(), calls=%async_computation.9 | async-start | bytes 1966080 | tf_op jit(solution)/shard_map/reduce_scatter | solution.py:45
  417.4 3.3 copy-start.5
  417.4 3.8 copy-start.7
  422.2 4.7 collective-permute-start.2
  425.5 5.5 %collective-permute-start.3 = (bf16[1,512]{1,0:T(2,128)(2,1)S(1)}, bf16[1,512]{1,0:T(2,128)(2,1)S(1)}, u32[]{:S(2)}, u32[]{:S(2)}) collective-permute-start(bf16[1,512]{1,0:T(2,128)(2,1)S(1)} %get-tuple-element.14), channel_id=1, source_target_pairs={{4,0},{8,4},{12,8},{5,1},{9,5},{13,9},{6,2},{10,6},{14,10},{7,3},{... | collective-permute-start | bytes 3080 | tf_op jit(solution)/shard_map/ppermute | solution.py:17
  431.1 32.8 %copy-start = (bf16[384,512]{1,0:T(8,128)(2,1)S(1)}, bf16[384,512]{1,0:T(8,128)(2,1)}, u32[]{:S(2)}) copy-start(bf16[384,512]{1,0:T(8,128)(2,1)} %add_convert_fusion.1) | copy-start | bytes 1179652
Sparse Core Ops, SparseCore 0:
  8.9 22.3 all-gather.6
  32.8 80.7 all-gather.12
  115.2 79.2 all-gather.10
  195.9 79.2 all-gather.14
  276.6 79.2 all-gather.8
  361.4 26.5 reduce-scatter.2
  397.1 20.2 all-gather.16
  436.8 27.1 reduce-scatter.4
where the time goes:
time: 480 us
  waiting for transfers between devices  419 us (87%)
  matrix products  20.6 us (4%)
  between operations  13.7 us (3%)
  blocking collectives  11.5 us (2%)
  starting transfers between devices  7.54 us (2%)
  other arithmetic  6.74 us (1%)
    all_gather x1, waiting for transfers between devices, shards(): lax.all_gather(value_weight, 'sp', axis=1, tiled=True)  82.3 us
    all_gather x1, waiting for transfers between devices, shards(): lax.all_gather(gate_weight, 'sp', axis=1, tiled=True)  80.7 us
    all_gather x1, waiting for transfers between devices, shards(): lax.all_gather(inner_weight, 'sp', axis=1, tiled=True)  77.8 us
    all_gather x1, waiting for transfers between devices, shards(): lax.all_gather(out_weight, 'sp', axis=2, tiled=True)  71.1 us
    reduce_scatter x2, waiting for transfers between devices, shards(): lax.psum_scatter(terms.astype(jnp.bfloat16), 'tp', scatter_dimension=1, t...  53.9 us
    all_gather x2, waiting for transfers between devices, shards(): whole = lax.all_gather(x, 'tp', axis=1, tiled=True)  41.6 us
    psum x2, blocking collectives, shards(): lax.psum((jnp.sum(total, axis=1), jnp.sum(total * total, axis=1)), 'tp')  11.5 us
    dot_general x2, matrix products, shards(): terms = jnp.dot(gated, full_out[layer], preferred_element_type=jnp.float32)  10.9 us
  transfers between devices with their start and end apart: 12, of which 10 were waited for; matrix products, arithmetic and copies ran while one was open for 1% of the time, Pallas kernels for 0%

commit v1 on v0

--- a/solution.py
+++ b/solution.py
@@ -29,7 +29,14 @@
         lax.all_gather(out_weight, "sp", axis=2, tiled=True),
     )
     for layer in range(LAYERS):
-        whole = lax.all_gather(x, "tp", axis=1, tiled=True)
+        ring = [x]
+        for hop in range(3):
+            ring.append(lax.ppermute(ring[-1], "tp", [(dev, (dev + 1) % 4) for dev in range(4)]))
+        whole = jnp.roll(
+            jnp.concatenate(ring[::-1], axis=1),
+            (lax.axis_index("tp") + 1) * ring[0].shape[1],
+            axis=1,
+        )
         outer = jnp.dot(whole, full_gate[layer], preferred_element_type=jnp.float32)
         inner = jnp.dot(whole, full_inner[layer], preferred_element_type=jnp.float32)
         values = jnp.dot(whole, full_value[layer], preferred_element_type=jnp.float32)

time: 480 us -> 461 us (0.960)
  waiting for transfers between devices: 419 us -> 397 us
    ppermute x0 -> x6, waiting for transfers between devices: none -> 43.3 us  [shards(): lax.ppermute(ring[-1], 'tp', [(dev, (dev + 1) % 4) for dev in range(4)])]
    all_gather x2 -> x0, waiting for transfers between devices: 41.6 us -> none  [shards(): whole = lax.all_gather(x, 'tp', axis=1, tiled=True)]
    all_gather x1, waiting for transfers between devices: 82.3 us -> 58.6 us  [shards(): lax.all_gather(value_weight, 'sp', axis=1, tiled=True)]
  transfers between devices with their start and end apart: 12 -> 16, of which waited for: 10 -> 14; matrix products, arithmetic and copies ran while one was open for 1% -> 2% of each run, Pallas kernels for 0% -> 0%
where the time goes in v1:
time: 461 us; the launch traced here: 460 us
  waiting for transfers between devices  397 us (86%)
  matrix products  17.8 us (4%)
  between operations  13.7 us (3%)
  blocking collectives  11.5 us (2%)
  other arithmetic  10.2 us (2%)
  starting transfers between devices  8.28 us (2%)
    all_gather x1, waiting for transfers between devices, shards(): lax.all_gather(gate_weight, 'sp', axis=1, tiled=True)  80.7 us
    all_gather x1, waiting for transfers between devices, shards(): lax.all_gather(inner_weight, 'sp', axis=1, tiled=True)  78.3 us
    all_gather x1, waiting for transfers between devices, shards(): lax.all_gather(out_weight, 'sp', axis=2, tiled=True)  71.3 us
    all_gather x1, waiting for transfers between devices, shards(): lax.all_gather(value_weight, 'sp', axis=1, tiled=True)  58.6 us
    reduce_scatter x2, waiting for transfers between devices, shards(): lax.psum_scatter(terms.astype(jnp.bfloat16), 'tp', scatter_dimension=1, t...  54.2 us
    ppermute x6, waiting for transfers between devices, shards(): lax.ppermute(ring[-1], 'tp', [(dev, (dev + 1) % 4) for dev in range(4)])  43.3 us
    psum x2, blocking collectives, shards(): lax.psum((jnp.sum(total, axis=1), jnp.sum(total * total, axis=1)), 'tp')  11.5 us
    dot_general x2, matrix products, shards(): terms = jnp.dot(gated, full_out[layer], preferred_element_type=jnp.float32)  10.7 us
  transfers between devices with their start and end apart: 16, of which 14 were waited for; matrix products, arithmetic and copies ran while one was open for 2% of the time, Pallas kernels for 0%

profile of v1, /device:TPU:0, one launch (start us, length us, event | category | flops | bytes accessed | tf_op | source)
XLA Modules:
  0.0 460.2 jit_solution(4481613327264194451)
XLA Ops:
  6.5 0.0 copy-start
  6.5 0.0 copy-start.1
  6.5 0.0 all-gather.9.cloned.1.call-start
  6.5 0.7 all-gather.9.cloned.1.call-update
  7.3 0.0 all-gather.7.cloned.1.call-start
  7.3 0.7 all-gather.7.cloned.1.call-update
  8.0 0.0 all-gather.11.cloned.1.call-start
  8.1 0.7 all-gather.11.cloned.1.call-update
  8.7 0.0 all-gather.5.cloned.1.call-start
  8.8 0.5 all-gather.5.cloned.1.call-update
  9.3 0.0 reduce-scatter.3.cloned.1.call-start
  9.4 0.0 copy-done
  9.4 0.5 collective-permute-start
  9.9 7.4 %collective-permute-done = bf16[384,512]{1,0:T(8,128)(2,1)S(1)} collective-permute-done((bf16[384,512]{1,0:T(8,128)(2,1)S(1)}, bf16[384,512]{1,0:T(8,128)(2,1)S(1)}, u32[]{:S(2)}, u32[]{:S(2)}) %collective-permute-start) | collective-permute-done | bytes 393248 | tf_op jit(solution)/shard_map/ppermute | solution.py:34
  17.3 0.0 collective-permute-start.1
  17.3 7.2 %collective-permute-done.1 = bf16[384,512]{1,0:T(8,128)(2,1)S(1)} collective-permute-done((bf16[384,512]{1,0:T(8,128)(2,1)S(1)}, bf16[384,512]{1,0:T(8,128)(2,1)S(1)}, u32[]{:S(2)}, u32[]{:S(2)}) %collective-permute-start.1) | collective-permute-done | bytes 393248 | tf_op jit(solution)/shard_map/ppermute | solution.py:34
  24.5 0.0 collective-permute-start.2
  24.5 0.0 copy-done.1
  24.5 7.2 %collective-permute-done.2 = bf16[384,512]{1,0:T(8,128)(2,1)S(1)} collective-permute-done((bf16[384,512]{1,0:T(8,128)(2,1)S(1)}, bf16[384,512]{1,0:T(8,128)(2,1)S(1)}, u32[]{:S(2)}, u32[]{:S(2)}) %collective-permute-start.2) | collective-permute-done | bytes 393248 | tf_op jit(solution)/shard_map/ppermute | solution.py:34
  31.7 2.0 fusion.16
  33.8 58.6 %all-gather.9.cloned.1.call-done = bf16[2,2048,512]{2,1,0:T(8,128)(2,1)} async-done(((bf16[2,512,512]{2,1,0:T(8,128)(2,1)}), bf16[2,2048,512]{2,1,0:T(8,128)(2,1)}) %all-gather.9.cloned.1.call-update) | async-done | bytes 4194320 | tf_op jit(solution)/shard_map/all_gather | solution.py:28
  92.4 2.6 fusion.29
  95.0 78.3 %all-gather.7.cloned.1.call-done = bf16[2,2048,512]{2,1,0:T(8,128)(2,1)} async-done(((bf16[2,512,512]{2,1,0:T(8,128)(2,1)}), bf16[2,2048,512]{2,1,0:T(8,128)(2,1)}) %all-gather.7.cloned.1.call-update) | async-done | bytes 4194320 | tf_op jit(solution)/shard_map/all_gather | solution.py:27
  173.2 2.6 fusion.27
  175.8 1.3 collective-permute-start.3
  177.1 1.3 collective-permute-start.4
  178.4 0.0 collective-permute-done.3
  178.4 4.2 collective-permute-done.4
  182.7 0.1 maximum_convert_fusion
  182.8 71.3 %all-gather.11.cloned.1.call-done = bf16[2,512,2048]{2,1,0:T(8,128)(2,1)} async-done(((bf16[2,512,512]{2,1,0:T(8,128)(2,1)}), bf16[2,512,2048]{2,1,0:T(8,128)(2,1)}) %all-gather.11.cloned.1.call-update) | async-done | bytes 4194320 | tf_op jit(solution)/shard_map/all_gather | solution.py:29
  254.1 80.7 %all-gather.5.cloned.1.call-done = bf16[2,2048,512]{2,1,0:T(8,128)(2,1)} async-done(((bf16[2,512,512]{2,1,0:T(8,128)(2,1)}), bf16[2,2048,512]{2,1,0:T(8,128)(2,1)}) %all-gather.5.cloned.1.call-update) | async-done | bytes 4194320 | tf_op jit(solution)/shard_map/all_gather | solution.py:26
  334.7 0.0 copy-start.2
  334.8 5.4 %convolution_convert_fusion.1 = bf16[384,2048]{1,0:T(8,128)(2,1)} fusion(bf16[2,512,2048]{2,1,0:T(8,128)(2,1)} %all-gather.11.cloned.1.call-done, bf16[384,2048]{1,0:T(8,128)(2,1)S(1)} %fusion.16, bf16[2,2048,512]{2,1,0:T(8,128)(2,1)} %all-gather.5.cloned.1.call-done, f32[386,512]{1,0:T(8,128)S(1)} %maximum_convert_fusion, f32[512]{0:T(512)S(1)} %bitcast.92, ...), kind=kOutput, calls=%fused_computation.17 | convolution fusion | flops 1613168640 | bytes 9705472 | tf_op jit(solution)/shard_map/dot_general | solution.py:51
  340.1 0.0 reduce-scatter.3.cloned.1.call-update
  340.1 0.0 reduce-scatter.5.cloned.1.call-start
  340.2 0.0 copy-done.2
  340.2 0.0 copy-done.3
  340.2 26.5 %reduce-scatter.3.cloned.1.call-done = bf16[384,512]{1,0:T(8,128)(2,1)} async-done(((bf16[384,2048]{1,0:T(8,128)(2,1)}), bf16[384,512]{1,0:T(8,128)(2,1)}) %reduce-scatter.3.cloned.1.call-update) | async-done | bytes 393232 | tf_op jit(solution)/shard_map/reduce_scatter | solution.py:52
  366.8 1.3 fusion.48
  368.0 5.8 %all-reduce.1 = (f32[384]{0:T(512)S(1)}, f32[384]{0:T(512)S(1)}) all-reduce(f32[384]{0:T(512)S(1)} %get-tuple-element.9, f32[384]{0:T(512)S(1)} %get-tuple-element.8), channel_id=1, replica_groups=mesh['grp'=2,'sp'=4,'tp'=4] {'tp'}, use_global_device_ids=true, to_apply=%region_4.6 | all-reduce | flops 768 | bytes 6144 | tf_op jit(solution)/shard_map/psum | solution.py:56
  373.8 1.4 add_convert_fusion.1
  375.2 0.1 collective-permute-start.5
  375.2 7.2 %collective-permute-done.5 = bf16[384,512]{1,0:T(8,128)(2,1)S(1)} collective-permute-done((bf16[384,512]{1,0:T(8,128)(2,1)S(1)}, bf16[384,512]{1,0:T(8,128)(2,1)S(1)}, u32[]{:S(2)}, u32[]{:S(2)}) %collective-permute-start.5) | collective-permute-done | bytes 393248 | tf_op jit(solution)/shard_map/ppermute | solution.py:34
  382.4 0.0 collective-permute-start.6
  382.4 7.2 %collective-permute-done.6 = bf16[384,512]{1,0:T(8,128)(2,1)S(1)} collective-permute-done((bf16[384,512]{1,0:T(8,128)(2,1)S(1)}, bf16[384,512]{1,0:T(8,128)(2,1)S(1)}, u32[]{:S(2)}, u32[]{:S(2)}) %collective-permute-start.6) | collective-permute-done | bytes 393248 | tf_op jit(solution)/shard_map/ppermute | solution.py:34
  389.6 0.0 collective-permute-start.7
  389.6 7.2 %collective-permute-done.7 = bf16[384,512]{1,0:T(8,128)(2,1)S(1)} collective-permute-done((bf16[384,512]{1,0:T(8,128)(2,1)S(1)}, bf16[384,512]{1,0:T(8,128)(2,1)S(1)}, u32[]{:S(2)}, u32[]{:S(2)}) %collective-permute-start.7) | collective-permute-done | bytes 393248 | tf_op jit(solution)/shard_map/ppermute | solution.py:34
  396.8 2.0 fusion.9
  398.9 0.0 copy-done.4
  398.9 0.0 copy-start.5
  398.9 1.0 fusion.39
  399.9 1.2 copy-done.5
  401.1 1.0 fusion.37
  402.1 3.6 collective-permute-start.8
  405.7 1.3 collective-permute-start.9
  407.0 0.0 collective-permute-done.8
  407.0 4.2 collective-permute-done.9
  411.2 0.1 maximum_convert_fusion.1
  411.3 5.4 %convolution_convert_fusion = bf16[384,2048]{1,0:T(8,128)(2,1)} fusion(bf16[2,512,2048]{2,1,0:T(8,128)(2,1)} %all-gather.11.cloned.1.call-done, bf16[384,2048]{1,0:T(8,128)(2,1)S(1)} %fusion.9, bf16[2,2048,512]{2,1,0:T(8,128)(2,1)} %all-gather.5.cloned.1.call-done, f32[386,512]{1,0:T(8,128)S(1)} %maximum_convert_fusion.1, f32[512]{0:T(512)S(1)} %bitcast.89, ...), kind=kOutput, calls=%fused_computation.16 | convolution fusion | flops 1613168640 | bytes 9705472 | tf_op jit(solution)/shard_map/dot_general | solution.py:51
  416.7 0.0 reduce-scatter.5.cloned.1.call-update
  416.7 27.6 %reduce-scatter.5.cloned.1.call-done = bf16[384,512]{1,0:T(8,128)(2,1)} async-done(((bf16[384,2048]{1,0:T(8,128)(2,1)}), bf16[384,512]{1,0:T(8,128)(2,1)}) %reduce-scatter.5.cloned.1.call-update) | async-done | bytes 393232 | tf_op jit(solution)/shard_map/reduce_scatter | solution.py:52
  444.3 1.3 fusion.49
  445.6 5.8 %all-reduce = (f32[384]{0:T(512)S(1)}, f32[384]{0:T(512)S(1)}) all-reduce(f32[384]{0:T(512)S(1)} %get-tuple-element.7, f32[384]{0:T(512)S(1)} %get-tuple-element.6), channel_id=1, replica_groups=mesh['grp'=2,'sp'=4,'tp'=4] {'tp'}, use_global_device_ids=true, to_apply=%region_9.11 | all-reduce | flops 768 | bytes 6144 | tf_op jit(solution)/shard_map/psum | solution.py:56
  451.3 2.0 add_convert_fusion
  (10 shorter events, 0.1 us)
Async XLA Ops:
  6.5 2.8 copy-start
  6.5 18.0 %copy-start.1 = (bf16[2,3,512]{2,0,1:T(2,128)(2,1)S(1)}, bf16[2,3,512]{2,0,1:T(2,128)(2,1)}, u32[]{:S(2)}) copy-start(bf16[2,3,512]{2,0,1:T(2,128)(2,1)} %param.15) | copy-start | bytes 18436
  6.5 85.9 %all-gather.9.cloned.1.call-start = ((), (), s32[]{:S(2)}) async-start(), calls=%async_computation.4 | async-start | bytes 5242880 | tf_op jit(solution)/shard_map/all_gather | solution.py:28
  7.3 166.0 %all-gather.7.cloned.1.call-start = ((), (), s32[]{:S(2)}) async-start(), calls=%async_computation.3 | async-start | bytes 5242880 | tf_op jit(solution)/shard_map/all_gather | solution.py:27
  8.0 246.1 %all-gather.11.cloned.1.call-start = ((), (), s32[]{:S(2)}) async-start(), calls=%async_computation.5 | async-start | bytes 5242880 | tf_op jit(solution)/shard_map/all_gather | solution.py:29
  8.7 326.0 %all-gather.5.cloned.1.call-start = ((), (), s32[]{:S(2)}) async-start(), calls=%async_computation.2 | async-start | bytes 5242880 | tf_op jit(solution)/shard_map/all_gather | solution.py:26
  9.3 357.4 %reduce-scatter.3.cloned.1.call-start = ((), (), s32[]{:S(2)}) async-start(), calls=%async_computation.6 | async-start | bytes 1966080 | tf_op jit(solution)/shard_map/reduce_scatter | solution.py:52
  9.4 7.9 %collective-permute-start = (bf16[384,512]{1,0:T(8,128)(2,1)S(1)}, bf16[384,512]{1,0:T(8,128)(2,1)S(1)}, u32[]{:S(2)}, u32[]{:S(2)}) collective-permute-start(bf16[384,512]{1,0:T(8,128)(2,1)S(1)} %copy-done), channel_id=1, source_target_pairs={{0,1},{1,2},{2,3},{3,0},{4,5},{5,6},{6,7},{7,4},{8,9},{9,10},{10,1... | collective-permute-start | bytes 1179656 | tf_op jit(solution)/shard_map/ppermute | solution.py:34
  17.3 7.2 %collective-permute-start.1 = (bf16[384,512]{1,0:T(8,128)(2,1)S(1)}, bf16[384,512]{1,0:T(8,128)(2,1)S(1)}, u32[]{:S(2)}, u32[]{:S(2)}) collective-permute-start(bf16[384,512]{1,0:T(8,128)(2,1)S(1)} %collective-permute-done), channel_id=1, source_target_pairs={{0,1},{1,2},{2,3},{3,0},{4,5},{5,6},{6,7},{7,4},{8,9},{9,10},{10,1... | collective-permute-start | bytes 1179656 | tf_op jit(solution)/shard_map/ppermute | solution.py:34
  24.5 7.2 %collective-permute-start.2 = (bf16[384,512]{1,0:T(8,128)(2,1)S(1)}, bf16[384,512]{1,0:T(8,128)(2,1)S(1)}, u32[]{:S(2)}, u32[]{:S(2)}) collective-permute-start(bf16[384,512]{1,0:T(8,128)(2,1)S(1)} %collective-permute-done.1), channel_id=1, source_target_pairs={{0,1},{1,2},{2,3},{3,0},{4,5},{5,6},{6,7},{7,4},{8,9},{9,10},{10,1... | collective-permute-start | bytes 1179656 | tf_op jit(solution)/shard_map/ppermute | solution.py:34
  175.8 2.6 collective-permute-start.3
  177.1 5.6 %collective-permute-start.4 = (bf16[1,512]{1,0:T(2,128)(2,1)S(1)}, bf16[1,512]{1,0:T(2,128)(2,1)S(1)}, u32[]{:S(2)}, u32[]{:S(2)}) collective-permute-start(bf16[1,512]{1,0:T(2,128)(2,1)S(1)} %get-tuple-element.17), channel_id=1, source_target_pairs={{4,0},{8,4},{12,8},{5,1},{9,5},{13,9},{6,2},{10,6},{14,10},{7,3},{... | collective-permute-start | bytes 3080 | tf_op jit(solution)/shard_map/ppermute | solution.py:17
  334.7 5.4 %copy-start.2 = (f32[2,512]{1,0:T(2,128)S(1)}, f32[2,512]{1,0:T(2,128)}, u32[]{:S(2)}) copy-start(f32[2,512]{1,0:T(2,128)} %param.16) | copy-start | bytes 12292
  334.8 5.5 %copy-start.3 = (f32[2,512]{1,0:T(2,128)S(1)}, f32[2,512]{1,0:T(2,128)}, u32[]{:S(2)}) copy-start(f32[2,512]{1,0:T(2,128)} %param.17) | copy-start | bytes 12292
  340.1 104.2 %reduce-scatter.5.cloned.1.call-start = ((), (), s32[]{:S(2)}) async-start(), calls=%async_computation.7 | async-start | bytes 1966080 | tf_op jit(solution)/shard_map/reduce_scatter | solution.py:52
  373.8 25.1 %copy-start.4 = (bf16[2,2048,512]{2,1,0:T(8,128)(2,1)S(1)}, bf16[2,2048,512]{2,1,0:T(8,128)(2,1)}, u32[]{:S(2)}) copy-start(bf16[2,2048,512]{2,1,0:T(8,128)(2,1)} %all-gather.9.cloned.1.call-done) | copy-start | bytes 12582916
  375.2 7.3 %collective-permute-start.5 = (bf16[384,512]{1,0:T(8,128)(2,1)S(1)}, bf16[384,512]{1,0:T(8,128)(2,1)S(1)}, u32[]{:S(2)}, u32[]{:S(2)}) collective-permute-start(bf16[384,512]{1,0:T(8,128)(2,1)S(1)} %add_convert_fusion.1), channel_id=1, source_target_pairs={{0,1},{1,2},{2,3},{3,0},{4,5},{5,6},{6,7},{7,4},{8,9},{9,10},{10,1... | collective-permute-start | bytes 1179656 | tf_op jit(solution)/shard_map/ppermute | solution.py:34
  382.4 7.2 %collective-permute-start.6 = (bf16[384,512]{1,0:T(8,128)(2,1)S(1)}, bf16[384,512]{1,0:T(8,128)(2,1)S(1)}, u32[]{:S(2)}, u32[]{:S(2)}) collective-permute-start(bf16[384,512]{1,0:T(8,128)(2,1)S(1)} %collective-permute-done.5), channel_id=1, source_target_pairs={{0,1},{1,2},{2,3},{3,0},{4,5},{5,6},{6,7},{7,4},{8,9},{9,10},{10,1... | collective-permute-start | bytes 1179656 | tf_op jit(solution)/shard_map/ppermute | solution.py:34
  389.6 7.2 %collective-permute-start.7 = (bf16[384,512]{1,0:T(8,128)(2,1)S(1)}, bf16[384,512]{1,0:T(8,128)(2,1)S(1)}, u32[]{:S(2)}, u32[]{:S(2)}) collective-permute-start(bf16[384,512]{1,0:T(8,128)(2,1)S(1)} %collective-permute-done.6), channel_id=1, source_target_pairs={{0,1},{1,2},{2,3},{3,0},{4,5},{5,6},{6,7},{7,4},{8,9},{9,10},{10,1... | collective-permute-start | bytes 1179656 | tf_op jit(solution)/shard_map/ppermute | solution.py:34
  398.9 2.2 copy-start.5
  402.1 4.9 %collective-permute-start.8 = (bf16[1,512]{1,0:T(2,128)(2,1)S(1)}, bf16[1,512]{1,0:T(2,128)(2,1)S(1)}, u32[]{:S(2)}, u32[]{:S(2)}) collective-permute-start(bf16[1,512]{1,0:T(2,128)(2,1)S(1)} %get-tuple-element.14), channel_id=1, source_target_pairs={{0,4},{4,8},{8,12},{1,5},{5,9},{9,13},{2,6},{6,10},{10,14},{3,7},{... | collective-permute-start | bytes 3080 | tf_op jit(solution)/shard_map/ppermute | solution.py:16
  405.7 5.5 %collective-permute-start.9 = (bf16[1,512]{1,0:T(2,128)(2,1)S(1)}, bf16[1,512]{1,0:T(2,128)(2,1)S(1)}, u32[]{:S(2)}, u32[]{:S(2)}) collective-permute-start(bf16[1,512]{1,0:T(2,128)(2,1)S(1)} %get-tuple-element.15), channel_id=1, source_target_pairs={{4,0},{8,4},{12,8},{5,1},{9,5},{13,9},{6,2},{10,6},{14,10},{7,3},{... | collective-permute-start | bytes 3080 | tf_op jit(solution)/shard_map/ppermute | solution.py:17
Sparse Core Ops, SparseCore 0:
  8.9 83.4 all-gather.8
  94.0 79.2 all-gather.6
  174.8 79.2 all-gather.10
  255.5 79.2 all-gather.4
  340.3 26.4 reduce-scatter.2
  416.8 27.4 reduce-scatter.4
